TPU v7x, 32 devices: a whole 2x2x4 slice. The times are simulated.
32 devices in a mesh: ep: 8 (over z, x), tp: 4 (over y, core).
Axes of the slice: x: 2, y: 2, z: 4, core: 2. Of those that a mesh axis runs over, the one named last changes fastest.
Arguments:
- residual: bfloat16 [512, 4096], P('ep', 'tp'), may hold values from -64 to 64
- routes: int32 [512, 2], P('ep'), may hold values from 0 to 7, all different within a row; in each aligned block of 64 rows (0 to 63, 64 to 127, ...) at most 32 rows name the same one
- route_weights: float32 [512, 2], P('ep'), may hold values from 0.2 to 1
- state_prev: float32 [512, 2, 64, 64], P('ep', None, 'tp'), may hold values from -6 to 6
- mix_gain: float32 [4096], replicated, may hold values from 0.1 to 1.9
- ffn_gain: float32 [4096], replicated, may hold values from 0.1 to 1.9
- w_in: bfloat16 [4096, 1024], P(None, 'tp'), may hold values from -0.09375 to 0.09375
- decay_rate: float32 [64, 64], P('tp'), may hold values from 0.5 to 8
- rotation: float32 [64, 64], P('tp'), may hold values from 0 to 200
- log_step: float32 [64], P('tp'), may hold values from -3.9 to -1.2
- in_re: float32 [64, 64, 16], P('tp'), may hold values from -1 to 1
- in_im: float32 [64, 64, 16], P('tp'), may hold values from -1 to 1
- read_re: float32 [64, 16, 64], P('tp'), may hold values from -0.5 to 0.5
- read_im: float32 [64, 16, 64], P('tp'), may hold values from -0.5 to 0.5
- skip_gain: float32 [64, 16], P('tp'), may hold values from -4 to 4
- w_glu: bfloat16 [1024, 1024], P(None, 'tp'), may hold values from -0.1875 to 0.1875
- w_out: bfloat16 [1024, 4096], P('tp'), may hold values from -0.1875 to 0.1875
- w_gate: bfloat16 [8, 4096, 5632], P('ep', None, 'tp'), may hold values from -0.09375 to 0.09375
- w_up: bfloat16 [8, 4096, 5632], P('ep', None, 'tp'), may hold values from -0.09375 to 0.09375
- w_down: bfloat16 [8, 5632, 4096], P('ep', 'tp'), may hold values from -0.078125 to 0.078125
Outputs:
- layer_out: bfloat16 [512, 4096], P('ep', 'tp')
- state_next: float32 [512, 2, 64, 64], P('ep', None, 'tp')
Inputs may be any that keep to these rules, and one draw needn't show every extreme that they name: `routes`: each row names 2 different experts. In each aligned block of 64 rows (the rows of one index of ep) no expert is named more than 32 times, a bound that some block reaches.
All inputs are finite; a program needn't handle non-finite values.
Results may differ from a plain program's by a relative error of at most 0.012.
Values may be sent and summed in bfloat16 or wider, within the bound.
A program may use at most 128 MiB of HBM per device.

v0:
```python
import functools
import types

import jax
import jax.numpy as jnp
from jax import lax
from jax.experimental import pallas as pl
from jax.experimental.pallas import tpu as pltpu
from jax.sharding import PartitionSpec as P

TOPK = 2
epsilon = 1e-06
MESH = pl.DeviceIdType.MESH


def remote(src, dst, send_sem, recv_sem, target):
    return pltpu.make_async_remote_copy(
        src_ref=src,
        dst_ref=dst,
        send_sem=send_sem,
        recv_sem=recv_sem,
        device_id=target,
        device_id_type=MESH,
    )


def columns(place, width):
    return pl.ds(pl.multiple_of(place * width, width), width)


def flipped(place, number):
    result, bit = place, 1
    while bit <= number:
        if number & bit:
            result = result + bit - 2 * bit * lax.rem(lax.div(place, bit), 2)
        bit *= 2
    return result


def visits(experts):
    near, far = max(experts // 4, 1), experts // 2
    here = list(range(near)) + list(range(far, far + far - near))
    return here + list(range(near, far)) + list(range(far + far - near, experts))


def batches(experts):
    return [(0, experts // 2), (experts // 2, experts)]


def earlier(count):
    row = lax.broadcasted_iota(jnp.int32, (count, count), 0)
    column = lax.broadcasted_iota(jnp.int32, (count, count), 1)
    return jnp.where(row < column, 1.0, 0.0).astype(jnp.bfloat16)


def route_maps(routes_t, weights_t, experts, capacity):
    tokens = routes_t.shape[1]
    lane = lax.broadcasted_iota(jnp.int32, (experts, tokens), 0)
    picks = [jnp.where(routes_t[k : k + 1, :] == lane, 1.0, 0.0) for k in range(TOPK)]
    every = sum(picks).astype(jnp.bfloat16)
    before = jnp.dot(every, earlier(tokens), preferred_element_type=jnp.float32)
    place = lax.broadcasted_iota(jnp.int32, (experts * capacity, tokens), 0)
    sent = jnp.zeros((experts * capacity, tokens), jnp.float32)
    weighted = sent
    for k in range(TOPK):
        slot = jnp.sum(before * picks[k], axis=0, keepdims=True).astype(jnp.int32)
        match = place == routes_t[k : k + 1, :] * capacity + slot
        sent = sent + jnp.where(match, 1.0, 0.0)
        weighted = weighted + jnp.where(match, weights_t[k : k + 1, :], 0.0)
    return sent.astype(jnp.bfloat16), weighted.T


def eigen_terms(rate_ref, rotation_ref, log_step_ref):
    groups = rate_ref.shape[0]
    row = lax.broadcasted_iota(jnp.int32, (groups, groups), 0)
    column = lax.broadcasted_iota(jnp.int32, (groups, groups), 1)
    diagonal = jnp.where(row == column, log_step_ref[...], 0.0)
    step_size = jnp.exp(jnp.sum(diagonal, axis=1, keepdims=True))
    real_part, rotation = -rate_ref[...], rotation_ref[...]
    magnitude = jnp.exp(real_part * step_size)
    decay_re = magnitude * jnp.cos(rotation * step_size)
    decay_im = magnitude * jnp.sin(rotation * step_size)
    denominator = real_part * real_part + rotation * rotation
    lift_re = ((decay_re - 1.0) * real_part + decay_im * rotation) / denominator
    lift_im = (decay_im * real_part - (decay_re - 1.0) * rotation) / denominator
    return decay_re, decay_im, lift_re, lift_im


def layer_kernel(chips, names, *refs):
    r = types.SimpleNamespace(**dict(zip(names, refs)))
    ep, tp = lax.axis_index("ep"), lax.axis_index("tp")
    resid_ref = r.residual
    tokens, width = resid_ref.shape
    experts, capacity, _ = r.outb.shape
    full, units = r.gate_w.shape
    channels = r.in_w.shape[1]
    groups, group_ch, states = r.b_re.shape
    members = 2 * chips
    groups_of = batches(experts)
    core, chip = lax.rem(tp, 2), lax.div(tp, 2)
    others = [lax.rem(chip + k, chips) for k in range(1, chips)]
    origin = [lax.rem(chip + chips - 1 - j, chips) for j in range(chips - 1)]
    twin = 2 * chip + 1 - core
    partner = (ep, twin)
    peers = [lax.rem(tp + k, members) for k in range(1, members)]
    order = visits(experts)
    place_of = [flipped(ep, k) for k in order]
    mine = columns(tp, width)
    stops = others + [chip]
    last = chips - 1
    sends = []

    def load(hbm, vmem, sem):
        copy = pltpu.make_async_copy(hbm, vmem, sem)
        copy.start()
        return copy

    barrier = pltpu.get_barrier_semaphore()
    greeted = [(e, tp) for e in place_of[1:]] + [(ep, p) for p in peers]
    for target in greeted:
        pl.semaphore_signal(barrier, inc=1, device_id=target, device_id_type=MESH)
    small = [
        load(r.b_re_hbm, r.b_re, r.small_sem.at[0]),
        load(r.b_im_hbm, r.b_im, r.small_sem.at[1]),
        load(r.c_re_hbm, r.c_re, r.small_sem.at[2]),
        load(r.c_im_hbm, r.c_im, r.small_sem.at[3]),
        load(r.state_hbm, r.state, r.small_sem.at[4]),
        load(r.in_hbm, r.in_w, r.small_sem.at[5]),
        load(r.glu_hbm, r.glu_w, r.small_sem.at[6]),
        load(r.out_hbm, r.out_w, r.small_sem.at[7]),
    ]
    span_2 = 2 * states
    r.drive_w[...] = jnp.zeros_like(r.drive_w)
    r.read_w[...] = jnp.zeros_like(r.read_w)
    for g in range(groups):
        r.skip_row[:, g * group_ch : (g + 1) * group_ch] = r.skip[g : g + 1, :]
    pl.semaphore_wait(barrier, len(greeted))

    def send(*parts):
        copy = remote(*parts)
        copy.start()
        sends.append(copy)

    def arrive(block, send_sem, recv_sem):
        remote(block, block, send_sem, recv_sem, partner).wait_recv()

    own_block = r.whole.at[tp]
    for j, y in enumerate(others):
        send(resid_ref, own_block, r.wide_send.at[j], r.wide_recv.at[j], (ep, 2 * y + core))
    send(resid_ref, own_block, r.twin_send.at[0], r.twin_recv.at[0], partner)
    spread, weight = route_maps(r.routes_t[...], r.weights_t[...], experts, capacity)
    r.spread[...] = spread
    r.weight[...] = weight
    decay_re, decay_im, lift_re, lift_im = eigen_terms(r.rate, r.rotation, r.log_step)

    def project(block, place):
        x = block.astype(jnp.float32)
        square = jnp.sum(x * x, axis=1, keepdims=True)
        x = (x * r.mix_gain[:, columns(place, width)]).astype(jnp.bfloat16)
        part = jnp.dot(x, r.in_w[columns(place, width), :], preferred_element_type=jnp.float32)
        return square, part

    for copy in small[:4]:
        copy.wait()
    for g in range(groups):
        one = slice(g, g + 1)
        rows_g = slice(g * group_ch, (g + 1) * group_ch)
        left = slice(g * span_2, g * span_2 + states)
        right = slice(g * span_2 + states, (g + 1) * span_2)
        in_re, in_im = r.b_re[g], r.b_im[g]
        map_re = lift_re[one] * in_re - lift_im[one] * in_im
        map_im = lift_re[one] * in_im + lift_im[one] * in_re
        r.drive_w[rows_g, left] = map_re.astype(jnp.bfloat16)
        r.drive_w[rows_g, right] = map_im.astype(jnp.bfloat16)
        r.read_w[rows_g, left] = r.c_re[g].astype(jnp.bfloat16)
        r.read_w[rows_g, right] = (-r.c_im[g]).astype(jnp.bfloat16)
    small[4].wait()
    stride = 2 * groups
    state_rows = [
        (pl.ds(g, tokens, stride=stride), pl.ds(groups + g, tokens, stride=stride))
        for g in range(groups)
    ]
    for g, (row_re, row_im) in enumerate(state_rows):
        one = slice(g, g + 1)
        old_re, old_im = r.state[row_re, :], r.state[row_im, :]
        r.fresh[:, g * span_2 : g * span_2 + states] = (
            decay_re[one] * old_re - decay_im[one] * old_im
        )
        r.fresh[:, g * span_2 + states : (g + 1) * span_2] = (
            decay_re[one] * old_im + decay_im[one] * old_re
        )
    small[5].wait()
    square, total = project(resid_ref[...], tp)
    arrive(r.whole.at[twin], r.twin_send.at[0], r.twin_recv.at[0])
    more = project(r.whole[twin], twin)
    square, total = square + more[0], total + more[1]
    for j, y in enumerate(origin):
        place = 2 * y + core
        arrive(r.whole.at[place], r.wide_send.at[j], r.wide_recv.at[j])
        block = r.whole.at[place]
        send(block, block, r.twin_send.at[1 + j], r.twin_recv.at[1 + j], partner)
        more = project(r.whole[place], place)
        square, total = square + more[0], total + more[1]
    for j, y in enumerate(origin):
        place = 2 * y + 1 - core
        arrive(r.whole.at[place], r.twin_send.at[1 + j], r.twin_recv.at[1 + j])
        more = project(r.whole[place], place)
        square, total = square + more[0], total + more[1]
    u_in = (total * lax.rsqrt(square / full + epsilon)).astype(jnp.bfloat16)

    loads = []
    pieces = r.load_sem.shape[1]
    pairs = ((r.gate_hbm, r.gate_w), (r.up_hbm, r.up_w), (r.down_hbm, r.down_w))
    for i, (hbm, vmem) in enumerate(pairs):
        step_rows = vmem.shape[0] // pieces
        for j in range(pieces):
            span = pl.ds(j * step_rows, step_rows)
            loads.append(load(hbm.at[0, span], vmem.at[span], r.load_sem.at[i, j]))
    drive = jnp.dot(u_in, r.drive_w[...], preferred_element_type=jnp.float32)
    new = r.fresh[...] + drive
    r.fresh[...] = new
    value = lax.dot_general(
        new.astype(jnp.bfloat16),
        r.read_w[...],
        (((1,), (1,)), ((), ())),
        preferred_element_type=jnp.float32,
    )
    act = jax.nn.gelu(value + r.skip_row[...] * u_in.astype(jnp.float32))
    r.acts[tp] = act.astype(jnp.bfloat16)
    for k, p in enumerate(peers):
        send(r.acts.at[tp], r.acts.at[tp], r.act_send.at[k], r.act_recv.at[k], (ep, p))
    for g, (row_re, row_im) in enumerate(state_rows):
        r.state_out[row_re, :] = r.fresh[:, g * span_2 : g * span_2 + states]
        r.state_out[row_im, :] = r.fresh[:, g * span_2 + states : (g + 1) * span_2]

    def gate_part(place):
        return jnp.dot(
            r.acts[place], r.glu_w[columns(place, channels), :], preferred_element_type=jnp.float32
        )

    small[6].wait()
    logit = gate_part(tp)
    for k in range(members - 1):
        place = lax.rem(tp + members - 1 - k, members)
        arrive(r.acts.at[place], r.act_send.at[k], r.act_recv.at[k])
        logit = logit + gate_part(place)
    mixed = (act * jax.nn.sigmoid(logit)).astype(jnp.bfloat16)

    small[7].wait()

    def branch(place):
        return jnp.dot(
            mixed, r.out_w[:, columns(place, width)], preferred_element_type=jnp.float32
        )

    def branch_near(i, y):
        r.b_part[i] = branch(2 * y + 1 - core).astype(jnp.bfloat16)
        send(r.b_part.at[i], r.b_near.at[i], r.b_near_send.at[i], r.b_near_recv.at[i], partner)

    for i, y in enumerate(others):
        branch_near(i, y)
    for i, y in enumerate(others):
        value = branch(2 * y + core)
        arrive(r.b_near.at[i], r.b_near_send.at[i], r.b_near_recv.at[i])
        r.b_staged[i] = (value + r.b_near[i].astype(jnp.float32)).astype(jnp.bfloat16)
        target = (ep, 2 * y + core)
        send(r.b_staged.at[i], r.b_far.at[i], r.b_far_send.at[i], r.b_far_recv.at[i], target)
    branch_near(last, chip)
    value = branch(tp)
    arrive(r.b_near.at[last], r.b_near_send.at[last], r.b_near_recv.at[last])
    value = value + r.b_near[last].astype(jnp.float32)
    for i in range(last):
        arrive(r.b_far.at[i], r.b_far_send.at[i], r.b_far_recv.at[i])
        value = value + r.b_far[i].astype(jnp.float32)
    after = (resid_ref[...].astype(jnp.float32) + value).astype(jnp.bfloat16)
    r.after[...] = after
    for e in range(experts):
        picked = r.spread[e * capacity : (e + 1) * capacity, :]
        block = jnp.dot(picked, after, preferred_element_type=jnp.float32)
        r.outb[e] = block.astype(jnp.bfloat16)

    for s in range(1, experts):
        e = place_of[s]
        send(r.outb.at[e], r.rows.at[s, :, mine], r.ep_send.at[s], r.ep_recv.at[s], (e, tp))
    r.rows[0, :, mine] = r.outb[ep]

    def forward(s):
        block = r.rows.at[s, :, mine]
        if s > 0:
            arrive(block, r.ep_send.at[s], r.ep_recv.at[s])
        for j, y in enumerate(others):
            send(block, block, r.fwd_send.at[s, j], r.fwd_recv.at[s, j], (ep, 2 * y + core))
        send(block, block, r.pair_send.at[s], r.pair_recv.at[s], partner)

    def relay(s):
        for j, y in enumerate(origin):
            block = r.rows.at[s, :, columns(2 * y + core, width)]
            arrive(block, r.fwd_send.at[s, j], r.fwd_recv.at[s, j])
            send(block, block, r.relay_send.at[s, j], r.relay_recv.at[s, j], partner)

    def norm(s):
        block = r.rows.at[s, :, columns(2 * chip + 1 - core, width)]
        arrive(block, r.pair_send.at[s], r.pair_recv.at[s])
        for j, y in enumerate(origin):
            block = r.rows.at[s, :, columns(2 * y + 1 - core, width)]
            arrive(block, r.relay_send.at[s, j], r.relay_recv.at[s, j])
        total = jnp.zeros((capacity, 128), jnp.float32)
        for c in range(full // 128):
            x = r.rows[s, :, c * 128 : (c + 1) * 128].astype(jnp.float32)
            total = total + x * x
        scale = lax.rsqrt(jnp.sum(total, axis=1, keepdims=True) / full + epsilon)
        first = s * capacity
        for c in range(full // 128):
            span = slice(c * 128, (c + 1) * 128)
            x = r.rows[s, :, span].astype(jnp.float32)
            x = x * scale * r.ffn_gain[:, span]
            r.normed[first : first + capacity, span] = x.astype(jnp.bfloat16)

    tile = 512
    chunks = [(at, min(tile, units - at)) for at in range(0, units, tile)]

    def gate_up(b, start, size):
        lo, hi = groups_of[b]
        count = (hi - lo) * capacity
        x, span = r.normed[lo * capacity : hi * capacity], slice(start, start + size)
        gate = jnp.dot(x, r.gate_w[:, span], preferred_element_type=jnp.float32)
        up = jnp.dot(x, r.up_w[:, span], preferred_element_type=jnp.float32)
        value = gate * jax.nn.sigmoid(gate) * up
        r.hidden[:count, span] = value.astype(jnp.bfloat16)

    def down(b, group):
        lo, hi = groups_of[b]
        span = columns(group, width)
        value = jnp.dot(
            r.hidden[: (hi - lo) * capacity],
            r.down_w[:, span],
            preferred_element_type=jnp.float32,
        )
        r.part[lo * capacity : hi * capacity, span] = value.astype(jnp.bfloat16)

    def near_out(b, i):
        lo, hi = groups_of[b]
        span = pl.ds(lo * capacity, (hi - lo) * capacity)
        send(
            r.part.at[span, columns(2 * stops[i] + 1 - core, width)],
            r.near.at[i, span],
            r.near_send.at[b, i],
            r.near_recv.at[b, i],
            partner,
        )

    def near_in(b, i):
        lo, hi = groups_of[b]
        block = r.near.at[i, pl.ds(lo * capacity, (hi - lo) * capacity)]
        arrive(block, r.near_send.at[b, i], r.near_recv.at[b, i])

    def leaving(b):
        inside = list(range(*groups_of[b]))
        first = experts // 4
        return inside[first:] + inside[:first][::-1]

    def far_out(b, i):
        y = others[i]
        near_in(b, i)
        for s in leaving(b):
            span = slice(s * capacity, (s + 1) * capacity)
            own = r.part[span, columns(2 * y + core, width)].astype(jnp.float32)
            summed_pair = own + r.near[i, span, :].astype(jnp.float32)
            r.staged[s, i] = summed_pair.astype(jnp.bfloat16)
            send(
                r.staged.at[s, i],
                r.far.at[s, i],
                r.far_send.at[s, i],
                r.far_recv.at[s, i],
                (ep, 2 * y + core),
            )

    def give_back(s):
        span = slice(s * capacity, (s + 1) * capacity)
        total = r.part[span, mine].astype(jnp.float32)
        total = total + r.near[last, span, :].astype(jnp.float32)
        for i in range(last):
            arrive(r.far.at[s, i], r.far_send.at[s, i], r.far_recv.at[s, i])
            total = total + r.far[s, i].astype(jnp.float32)
        if s == 0:
            r.back[ep] = total.astype(jnp.bfloat16)
        else:
            r.summed[s] = total.astype(jnp.bfloat16)
            send(
                r.summed.at[s],
                r.back.at[ep],
                r.back_send.at[s],
                r.back_recv.at[s],
                (place_of[s], tp),
            )

    def run_batch(b, events):
        def step():
            for event in events.pop(0) if events else ():
                event()

        for start, size in chunks:
            gate_up(b, start, size)
            step()
        if b == 0:
            for copy in loads[2 * pieces :]:
                copy.wait()
        for i in range(chips):
            down(b, 2 * stops[i] + 1 - core)
            near_out(b, i)
        step()
        for i in range(last):
            down(b, 2 * stops[i] + core)
            far_out(b, i)
        step()
        down(b, tp)
        near_in(b, last)
        while events:
            step()

    def act_on(what, *slots):
        return [functools.partial(what, s) for s in slots]

    def spread_out(events, points):
        share = -(-len(events) // points)
        return [events[at : at + share] for at in range(0, len(events), share)]

    half, early = experts // 2, experts // 2 + experts // 4
    for s in range(early):
        forward(s)
        if 2 <= s < half + 2:
            relay(s - 2)
    for s in range(half):
        norm(s)
    for copy in loads[: 2 * pieces]:
        copy.wait()
    points = len(chunks) + 3
    events = act_on(forward, *range(early, experts)) + act_on(relay, *range(half, experts - 1))
    run_batch(0, spread_out(events, points))
    for s in range(half, early):
        norm(s)
    relay(experts - 1)
    for s in range(early, experts):
        norm(s)
    run_batch(1, spread_out(act_on(give_back, *leaving(0)), points))
    for s in leaving(1):
        give_back(s)
    for s in range(1, experts):
        landed = r.back.at[place_of[s]]
        arrive(landed, r.back_send.at[s], r.back_recv.at[s])
    weight = r.weight[...]
    coarse = weight.astype(jnp.bfloat16)
    fine = (weight - coarse.astype(jnp.float32)).astype(jnp.bfloat16)
    returned = r.back[...].reshape(experts * capacity, width)
    combined = jnp.dot(coarse, returned, preferred_element_type=jnp.float32)
    combined = combined + jnp.dot(fine, returned, preferred_element_type=jnp.float32)
    r.layer_out[...] = (r.after[...].astype(jnp.float32) + combined).astype(jnp.bfloat16)
    for copy in sends:
        copy.wait_send()


def run_layer(values, weights, experts, chips):
    residual, state = values["residual"], values["state_hbm"]
    tokens, width = residual.shape
    full, channels = weights["in_hbm"].shape
    units = weights["gate_hbm"].shape[2]
    groups, group_ch, states = weights["b_re_hbm"].shape
    capacity = 2 * tokens * TOPK // experts
    hops, members, pieces = chips - 1, 2 * chips, 4
    most = max(hi - lo for lo, hi in batches(experts)) * capacity
    dma, bf16, f32 = pltpu.SemaphoreType.DMA, jnp.bfloat16, jnp.float32
    scratch = dict(
        in_w=pltpu.VMEM((full, channels), bf16),
        state=pltpu.VMEM(state.shape, f32),
        fresh=pltpu.VMEM((tokens, 2 * groups * states), f32),
        drive_w=pltpu.VMEM((channels, 2 * groups * states), bf16),
        read_w=pltpu.VMEM((channels, 2 * groups * states), bf16),
        skip_row=pltpu.VMEM((1, channels), f32),
        b_re=pltpu.VMEM((groups, group_ch, states), f32),
        b_im=pltpu.VMEM((groups, group_ch, states), f32),
        c_re=pltpu.VMEM((groups, group_ch, states), f32),
        c_im=pltpu.VMEM((groups, group_ch, states), f32),
        glu_w=pltpu.VMEM((channels * members, channels), bf16),
        out_w=pltpu.VMEM((channels, full), bf16),
        gate_w=pltpu.VMEM((full, units), bf16),
        up_w=pltpu.VMEM((full, units), bf16),
        down_w=pltpu.VMEM((units, full), bf16),
        whole=pltpu.VMEM((members, tokens, width), bf16),
        acts=pltpu.VMEM((members, tokens, channels), bf16),
        b_part=pltpu.VMEM((chips, tokens, width), bf16),
        b_near=pltpu.VMEM((chips, tokens, width), bf16),
        b_staged=pltpu.VMEM((hops, tokens, width), bf16),
        b_far=pltpu.VMEM((hops, tokens, width), bf16),
        after=pltpu.VMEM((tokens, width), bf16),
        spread=pltpu.VMEM((experts * capacity, tokens), bf16),
        weight=pltpu.VMEM((tokens, experts * capacity), f32),
        outb=pltpu.VMEM((experts, capacity, width), bf16),
        rows=pltpu.VMEM((experts, capacity, full), bf16),
        normed=pltpu.VMEM((experts * capacity, full), bf16),
        hidden=pltpu.VMEM((most, units), bf16),
        part=pltpu.VMEM((experts * capacity, full), bf16),
        near=pltpu.VMEM((chips, experts * capacity, width), bf16),
        staged=pltpu.VMEM((experts, hops, capacity, width), bf16),
        far=pltpu.VMEM((experts, hops, capacity, width), bf16),
        summed=pltpu.VMEM((experts, capacity, width), bf16),
        back=pltpu.VMEM((experts, capacity, width), bf16),
        small_sem=dma((9,)),
        load_sem=dma((3, pieces)),
    )
    for name, shape in dict(
        wide=(hops,),
        twin=(chips,),
        act=(members - 1,),
        b_near=(chips,),
        b_far=(hops,),
        ep=(experts,),
        pair=(experts,),
        fwd=(experts, hops),
        relay=(experts, hops),
        near=(2, chips),
        far=(experts, hops),
        back=(experts,),
    ).items():
        scratch[name + "_send"] = dma(shape)
        scratch[name + "_recv"] = dma(shape)
    operands = {**values, **weights}
    vmem, hbm = pl.BlockSpec(memory_space=pltpu.VMEM), pl.BlockSpec(memory_space=pl.ANY)
    names = list(operands) + ["layer_out", "state_out"] + list(scratch)
    return pl.pallas_call(
        functools.partial(layer_kernel, chips, names),
        out_shape=(pltpu.VMEM(residual.shape, bf16), pltpu.VMEM(state.shape, f32)),
        in_specs=[hbm if name.endswith("_hbm") else vmem for name in operands],
        out_specs=(vmem, vmem),
        scratch_shapes=list(scratch.values()),
        compiler_params=pltpu.CompilerParams(
            collective_id=0, has_side_effects=True, vmem_limit_bytes=58 * 2**20
        ),
        name="layer",
    )(*operands.values())


def per_device(
    residual,
    routes,
    route_weights,
    state_prev,
    mix_gain,
    ffn_gain,
    w_in,
    decay_rate,
    rotation,
    log_step,
    in_re,
    in_im,
    read_re,
    read_im,
    skip_gain,
    w_glu,
    w_out,
    w_gate,
    w_up,
    w_down,
):
    values = dict(
        residual=residual,
        routes_t=routes.T,
        weights_t=route_weights.T,
        mix_gain=mix_gain[None, :],
        ffn_gain=ffn_gain[None, :],
        rate=decay_rate,
        rotation=rotation,
        log_step=log_step[None, :],
        skip=skip_gain,
        state_hbm=state_prev.reshape(-1, state_prev.shape[-1]),
    )
    weights = dict(
        in_hbm=w_in,
        b_re_hbm=jnp.swapaxes(in_re, 1, 2),
        b_im_hbm=jnp.swapaxes(in_im, 1, 2),
        c_re_hbm=read_re,
        c_im_hbm=read_im,
        glu_hbm=w_glu,
        out_hbm=w_out,
        gate_hbm=w_gate,
        up_hbm=w_up,
        down_hbm=w_down,
    )
    layer_out, state_next = run_layer(
        values, weights, lax.axis_size("ep"), lax.axis_size("tp") // 2
    )
    return (layer_out, state_next.reshape(state_prev.shape))


def solution(mesh):
    return jax.shard_map(
        per_device,
        mesh=mesh,
        in_specs=(
            P("ep", "tp"),
            P("ep", None),
            P("ep", None),
            P("ep", None, "tp", None),
            P(),
            P(),
            P(None, "tp"),
            P("tp", None),
            P("tp", None),
            P("tp"),
            P("tp", None, None),
            P("tp", None, None),
            P("tp", None, None),
            P("tp", None, None),
            P("tp", None),
            P(None, "tp"),
            P("tp", None),
            P("ep", None, "tp"),
            P("ep", None, "tp"),
            P("ep", "tp", None),
        ),
        out_specs=(P("ep", "tp"), P("ep", None, "tp", None)),
        check_vma=False,
    )
```

profile of v0, /device:TPU:0, one launch (start us, length us, event | category | flops | bytes accessed | tf_op | source)
XLA Modules:
  0.0 66.1 jit_solution(6481930105217467905)
XLA Ops:
  0.6 63.8 %layer.1 = (bf16[64,1024]{1,0:T(8,128)(2,1)S(1)}, f32[2048,64]{1,0:T(8,128)S(1)}) custom-call(bf16[64,1024]{1,0:T(8,128)(2,1)} %refs_0_.1, s32[2,64]{1,0:T(2,128)} %bitcast.15, f32[2,64]{1,0:T(2,128)} %bitcast.16, f32[1,4096]{1,0:T(1,128)} %bitcast.13, f32[1,4096]{1,0:T(1,128)} %bitcast.14, f32[16,64]{1,0:T(8,128)} %refs_5_.1, f32[16,64]{1,0:T(8,128)} %refs_6_.1, ...), custom_call_target="tpu_custom_call" | custom-call | tf_op jit(solution)/shard_map/layer/pallas_call | solution.py:529
  64.5 0.7 copy.24
  65.1 1.0 %copy.25 = f32[64,2,16,64]{3,2,1,0:T(8,128)} copy(f32[64,2,16,64]{3,2,1,0:T(8,128)S(1)} %bitcast.9) | data formatting | bytes 1048576
where the time goes:
time: 66.2 us; the launch traced here: 66.1 us
  Pallas kernels  63.8 us (96%)
  local copies, waits for them, and re-layouts  1.63 us (2%)
    pallas_call x1, Pallas kernels, run_layer(): pl.pallas_call(functools.partial(layer_kernel, chips, names), out_shape=(...  63.8 us
    unnamed x2, local copies, waits for them, and re-layouts  1.63 us

commit v1 on v0

--- a/solution.py
+++ b/solution.py
@@ -9,6 +9,16 @@
 from jax.sharding import PartitionSpec as P
 
 TOPK = 2
+TINY = [
+    "routes_t",
+    "weights_t",
+    "mix_gain",
+    "ffn_gain",
+    "rate",
+    "rotation",
+    "log_step",
+    "skip",
+]
 epsilon = 1e-06
 MESH = pl.DeviceIdType.MESH
 
@@ -119,6 +129,11 @@
     greeted = [(e, tp) for e in place_of[1:]] + [(ep, p) for p in peers]
     for target in greeted:
         pl.semaphore_signal(barrier, inc=1, device_id=target, device_id_type=MESH)
+    lead = load(r.residual_hbm, r.residual, r.lead_sem.at[0])
+    tiny = [
+        load(getattr(r, name + "_hbm"), getattr(r, name), r.lead_sem.at[1 + at])
+        for at, name in enumerate(TINY)
+    ]
     small = [
         load(r.b_re_hbm, r.b_re, r.small_sem.at[0]),
         load(r.b_im_hbm, r.b_im, r.small_sem.at[1]),
@@ -132,8 +147,6 @@
     span_2 = 2 * states
     r.drive_w[...] = jnp.zeros_like(r.drive_w)
     r.read_w[...] = jnp.zeros_like(r.read_w)
-    for g in range(groups):
-        r.skip_row[:, g * group_ch : (g + 1) * group_ch] = r.skip[g : g + 1, :]
     pl.semaphore_wait(barrier, len(greeted))
 
     def send(*parts):
@@ -144,10 +157,13 @@
     def arrive(block, send_sem, recv_sem):
         remote(block, block, send_sem, recv_sem, partner).wait_recv()
 
+    lead.wait()
     own_block = r.whole.at[tp]
     for j, y in enumerate(others):
         send(resid_ref, own_block, r.wide_send.at[j], r.wide_recv.at[j], (ep, 2 * y + core))
     send(resid_ref, own_block, r.twin_send.at[0], r.twin_recv.at[0], partner)
+    for copy in tiny:
+        copy.wait()
     spread, weight = route_maps(r.routes_t[...], r.weights_t[...], experts, capacity)
     r.spread[...] = spread
     r.weight[...] = weight
@@ -162,6 +178,8 @@
 
     for copy in small[:4]:
         copy.wait()
+    for g in range(groups):
+        r.skip_row[:, g * group_ch : (g + 1) * group_ch] = r.skip[g : g + 1, :]
     for g in range(groups):
         one = slice(g, g + 1)
         rows_g = slice(g * group_ch, (g + 1) * group_ch)
@@ -248,31 +266,52 @@
 
     small[7].wait()
 
-    def branch(place):
-        return jnp.dot(
-            mixed, r.out_w[:, columns(place, width)], preferred_element_type=jnp.float32
-        )
+    cut = width // 2
+    cuts = [slice(0, cut), slice(cut, width)]
+
+    def branch(place, q):
+        span = pl.ds(pl.multiple_of(place * width + q * cut, cut), cut)
+        return jnp.dot(mixed, r.out_w[:, span], preferred_element_type=jnp.float32)
 
     def branch_near(i, y):
-        r.b_part[i] = branch(2 * y + 1 - core).astype(jnp.bfloat16)
-        send(r.b_part.at[i], r.b_near.at[i], r.b_near_send.at[i], r.b_near_recv.at[i], partner)
+        for q, span in enumerate(cuts):
+            r.b_part[i, :, span] = branch(2 * y + 1 - core, q).astype(jnp.bfloat16)
+            send(
+                r.b_part.at[i, :, span],
+                r.b_near.at[i, :, span],
+                r.b_near_send.at[i, q],
+                r.b_near_recv.at[i, q],
+                partner,
+            )
+
+    def branch_sum(i, y, q):
+        value = branch(2 * y + core, q)
+        block = r.b_near.at[i, :, cuts[q]]
+        arrive(block, r.b_near_send.at[i, q], r.b_near_recv.at[i, q])
+        return value + r.b_near[i, :, cuts[q]].astype(jnp.float32)
 
     for i, y in enumerate(others):
         branch_near(i, y)
     for i, y in enumerate(others):
-        value = branch(2 * y + core)
-        arrive(r.b_near.at[i], r.b_near_send.at[i], r.b_near_recv.at[i])
-        r.b_staged[i] = (value + r.b_near[i].astype(jnp.float32)).astype(jnp.bfloat16)
-        target = (ep, 2 * y + core)
-        send(r.b_staged.at[i], r.b_far.at[i], r.b_far_send.at[i], r.b_far_recv.at[i], target)
+        for q, span in enumerate(cuts):
+            r.b_staged[i, :, span] = branch_sum(i, y, q).astype(jnp.bfloat16)
+            send(
+                r.b_staged.at[i, :, span],
+                r.b_far.at[i, :, span],
+                r.b_far_send.at[i, q],
+                r.b_far_recv.at[i, q],
+                (ep, 2 * y + core),
+            )
     branch_near(last, chip)
-    value = branch(tp)
-    arrive(r.b_near.at[last], r.b_near_send.at[last], r.b_near_recv.at[last])
-    value = value + r.b_near[last].astype(jnp.float32)
+    for q, span in enumerate(cuts):
+        r.after_sum[:, span] = resid_ref[:, span].astype(jnp.float32) + branch_sum(last, chip, q)
+    value = r.after_sum[...]
     for i in range(last):
-        arrive(r.b_far.at[i], r.b_far_send.at[i], r.b_far_recv.at[i])
+        for q, span in enumerate(cuts):
+            block = r.b_far.at[i, :, span]
+            arrive(block, r.b_far_send.at[i, q], r.b_far_recv.at[i, q])
         value = value + r.b_far[i].astype(jnp.float32)
-    after = (resid_ref[...].astype(jnp.float32) + value).astype(jnp.bfloat16)
+    after = value.astype(jnp.bfloat16)
     r.after[...] = after
     for e in range(experts):
         picked = r.spread[e * capacity : (e + 1) * capacity, :]
@@ -316,7 +355,7 @@
             x = x * scale * r.ffn_gain[:, span]
             r.normed[first : first + capacity, span] = x.astype(jnp.bfloat16)
 
-    tile = 512
+    tile = 256
     chunks = [(at, min(tile, units - at)) for at in range(0, units, tile)]
 
     def gate_up(b, start, size):
@@ -399,9 +438,10 @@
             for event in events.pop(0) if events else ():
                 event()
 
-        for start, size in chunks:
+        for at, (start, size) in enumerate(chunks):
             gate_up(b, start, size)
-            step()
+            if at in pauses[b]:
+                step()
         if b == 0:
             for copy in loads[2 * pieces :]:
                 copy.wait()
@@ -434,15 +474,13 @@
         norm(s)
     for copy in loads[: 2 * pieces]:
         copy.wait()
-    points = len(chunks) + 3
-    events = act_on(forward, *range(early, experts)) + act_on(relay, *range(half, experts - 1))
-    run_batch(0, spread_out(events, points))
-    for s in range(half, early):
+    pauses = ({len(chunks) // 3}, {len(chunks) - 1})
+    events = spread_out(act_on(relay, *range(half, experts - 1)), 3)
+    run_batch(0, [act_on(forward, *range(early, experts))] + events)
+    relay(experts - 1)
+    for s in range(half, experts):
         norm(s)
-    relay(experts - 1)
-    for s in range(early, experts):
-        norm(s)
-    run_batch(1, spread_out(act_on(give_back, *leaving(0)), points))
+    run_batch(1, [[]] + spread_out(act_on(give_back, *leaving(0)), 2))
     for s in leaving(1):
         give_back(s)
     for s in range(1, experts):
@@ -460,7 +498,8 @@
 
 
 def run_layer(values, weights, experts, chips):
-    residual, state = values["residual"], values["state_hbm"]
+    values = {name if name == "state_hbm" else name + "_hbm": a for name, a in values.items()}
+    residual, state = values["residual_hbm"], values["state_hbm"]
     tokens, width = residual.shape
     full, channels = weights["in_hbm"].shape
     units = weights["gate_hbm"].shape[2]
@@ -469,7 +508,11 @@
     hops, members, pieces = chips - 1, 2 * chips, 4
     most = max(hi - lo for lo, hi in batches(experts)) * capacity
     dma, bf16, f32 = pltpu.SemaphoreType.DMA, jnp.bfloat16, jnp.float32
-    scratch = dict(
+    scratch = {
+        name: pltpu.VMEM(values[name + "_hbm"].shape, values[name + "_hbm"].dtype)
+        for name in ["residual"] + TINY
+    }
+    scratch.update(
         in_w=pltpu.VMEM((full, channels), bf16),
         state=pltpu.VMEM(state.shape, f32),
         fresh=pltpu.VMEM((tokens, 2 * groups * states), f32),
@@ -491,6 +534,7 @@
         b_near=pltpu.VMEM((chips, tokens, width), bf16),
         b_staged=pltpu.VMEM((hops, tokens, width), bf16),
         b_far=pltpu.VMEM((hops, tokens, width), bf16),
+        after_sum=pltpu.VMEM((tokens, width), f32),
         after=pltpu.VMEM((tokens, width), bf16),
         spread=pltpu.VMEM((experts * capacity, tokens), bf16),
         weight=pltpu.VMEM((tokens, experts * capacity), f32),
@@ -504,15 +548,16 @@
         far=pltpu.VMEM((experts, hops, capacity, width), bf16),
         summed=pltpu.VMEM((experts, capacity, width), bf16),
         back=pltpu.VMEM((experts, capacity, width), bf16),
-        small_sem=dma((9,)),
+        lead_sem=dma((1 + len(TINY),)),
+        small_sem=dma((8,)),
         load_sem=dma((3, pieces)),
     )
     for name, shape in dict(
         wide=(hops,),
         twin=(chips,),
         act=(members - 1,),
-        b_near=(chips,),
-        b_far=(hops,),
+        b_near=(chips, 2),
+        b_far=(hops, 2),
         ep=(experts,),
         pair=(experts,),
         fwd=(experts, hops),
@@ -537,6 +582,30 @@
         ),
         name="layer",
     )(*operands.values())
+
+
+def store_kernel(count, *refs):
+    sems = refs[-1]
+    copies = [
+        pltpu.make_async_copy(refs[i], refs[count + i], sems.at[i]) for i in range(count)
+    ]
+    for copy in copies:
+        copy.start()
+    for copy in copies:
+        copy.wait()
+
+
+def store(*arrays):
+    vmem, hbm = pl.BlockSpec(memory_space=pltpu.VMEM), pl.BlockSpec(memory_space=pl.ANY)
+    held = [pltpu.with_memory_space_constraint(a, pltpu.VMEM) for a in arrays]
+    return pl.pallas_call(
+        functools.partial(store_kernel, len(arrays)),
+        out_shape=tuple(jax.ShapeDtypeStruct(a.shape, a.dtype) for a in arrays),
+        in_specs=[vmem] * len(arrays),
+        out_specs=(hbm,) * len(arrays),
+        scratch_shapes=[pltpu.SemaphoreType.DMA((len(arrays),))],
+        name="store",
+    )(*held)
 
 
 def per_device(
@@ -588,6 +657,7 @@
     layer_out, state_next = run_layer(
         values, weights, lax.axis_size("ep"), lax.axis_size("tp") // 2
     )
+    layer_out, state_next = store(layer_out, state_next)
     return (layer_out, state_next.reshape(state_prev.shape))
 
 

time: 66.2 us -> 63.9 us (0.965)
  local copies, waits for them, and re-layouts: 1.63 us -> 0 us
  Pallas kernels: 63.8 us -> 63 us
    pallas_call x1, Pallas kernels: 63.8 us -> 61.9 us  [run_layer(): pl.pallas_call(functools.partial(layer_kernel, chips, names), out_shape=(...]
    unnamed x2 -> x0, local copies, waits for them, and re-layouts: 1.63 us -> none
    pallas_call x0 -> x1, Pallas kernels: none -> 1.03 us  [store(): pl.pallas_call(functools.partial(store_kernel, len(arrays)), out_shape=tu...]
where the time goes in v1:
time: 63.9 us; the launch traced here: 63.8 us
  Pallas kernels  63 us (99%)
  between operations  0.81 us (1%)
    pallas_call x1, Pallas kernels, run_layer(): pl.pallas_call(functools.partial(layer_kernel, chips, names), out_shape=(...  61.9 us

profile of v1, /device:TPU:0, one launch (start us, length us, event | category | flops | bytes accessed | tf_op | source)
XLA Modules:
  0.0 63.8 jit_solution(15595701310423575919)
XLA Ops:
  0.6 61.9 %layer.1 = (bf16[64,1024]{1,0:T(8,128)(2,1)S(1)}, f32[2048,64]{1,0:T(8,128)S(1)}) custom-call(bf16[64,1024]{1,0:T(8,128)(2,1)} %refs_0_.1, s32[2,64]{1,0:T(2,128)} %bitcast.14, f32[2,64]{1,0:T(2,128)} %bitcast.15, f32[1,4096]{1,0:T(1,128)} %bitcast.12, f32[1,4096]{1,0:T(1,128)} %bitcast.13, f32[16,64]{1,0:T(8,128)} %refs_5_.1, f32[16,64]{1,0:T(8,128)} %refs_6_.1, ...), custom_call_target="tpu_custom_call" | custom-call | tf_op jit(solution)/shard_map/layer/pallas_call | solution.py:574
  62.6 1.0 %store.1 = (bf16[64,1024]{1,0:T(8,128)(2,1)}, f32[2048,64]{1,0:T(8,128)}) custom-call(bf16[64,1024]{1,0:T(8,128)(2,1)S(1)} %get-tuple-element.6.refs_0_, f32[2048,64]{1,0:T(8,128)S(1)} %get-tuple-element.7.refs_1_), custom_call_target="tpu_custom_call" | custom-call | tf_op jit(solution)/shard_map/store/pallas_call | solution.py:601
